TPU v7x, 512 devices: a whole 4x4x16 slice. The times are simulated.
512 devices in a mesh: sp: 32 (over z, core), tp: 16 (over y, x).
Axes of the slice: x: 4, y: 4, z: 16, core: 2. Of those that a mesh axis runs over, the one named last changes fastest.
Arguments:
- rec_input: bfloat16 [12288, 3072], P('sp', 'tp'), may hold values from -6 to 6
- gate_input: bfloat16 [12288, 3072], P('sp', 'tp'), may hold values from -6 to 6
- conv_weight: bfloat16 [4, 3072], P(None, 'tp'), may hold values from -3 to 3
- decay_wide: bfloat16 [2, 16, 128, 128], P(None, 'tp'), may hold values from -0.5 to 0.5
- decay_narrow: bfloat16 [2, 16, 64, 64], P(None, 'tp'), may hold values from -0.75 to 0.75
- input_wide: bfloat16 [2, 16, 128, 128], P(None, 'tp'), may hold values from -0.5 to 0.5
- input_narrow: bfloat16 [2, 16, 64, 64], P(None, 'tp'), may hold values from -0.75 to 0.75
- decay_base: float32 [2, 3072], P(None, 'tp'), may hold values from 1.6276042e-06 to 2.0345053e-05
- decay_extra: float32 [2, 12288, 2, 16], P(None, 'sp', None, 'tp'), may hold values from -1 to 0
- tokens: bfloat16 [12288, 2048], P('sp', 'tp'), may hold values from -16 to 16
- out_weight: bfloat16 [3072, 2048], P(None, 'tp'), may hold values from -0.3125 to 0.3125
- norm_gain: float32 [2048], P('tp'), may hold values from 0.1 to 1.9
- shared_gate: bfloat16 [2048, 2048], P(None, 'tp'), may hold values from -0.125 to 0.125
- shared_up: bfloat16 [2048, 2048], P(None, 'tp'), may hold values from -0.125 to 0.125
- shared_down: bfloat16 [2048, 2048], P(None, 'tp'), may hold values from -0.125 to 0.125
- expert_gate: bfloat16 [32, 2048, 2048], P('sp', None, 'tp'), may hold values from -0.125 to 0.125
- expert_up: bfloat16 [32, 2048, 2048], P('sp', None, 'tp'), may hold values from -0.125 to 0.125
- expert_down: bfloat16 [32, 2048, 2048], P('sp', None, 'tp'), may hold values from -0.125 to 0.125
- routes: int32 [12288, 2], P('sp'), may hold values from 0 to 31, all different within a row; in each aligned block of 384 rows (0 to 383, 384 to 767, ...) at most 36 rows name the same one
- route_weight: float32 [12288, 2], P('sp'), may hold values from 0.2 to 1.5
Outputs:
- layer_out: bfloat16 [12288, 2048], P('sp', 'tp')
Inputs may be any that keep to these rules, and one draw needn't show every extreme that they name: `routes`: each row names 2 different experts. The rows of one index of sp name no expert more than 36 times, and in some such block one expert exactly 36 times.
All inputs are finite; a program needn't handle non-finite values.
Results may differ from a plain program's by a relative error of at most 0.0052.
Values may be sent and summed in bfloat16 or wider, within the bound.
A program may use at most 64 MiB of HBM per device.

v0:
```python
import functools

import jax
import jax.numpy as jnp
from jax import lax
from jax.experimental import pallas as pl
from jax.experimental.pallas import tpu as pltpu
from jax.sharding import PartitionSpec as P

MESH = pl.DeviceIdType.MESH
BF = jnp.bfloat16
F32 = jnp.float32
D = 2048
NORM_EPS = 1e-06
RATE_SCALE = 8.0
NSP = 32
NTP = 16
TOK = 384
CH = 192
WIDE = 128
STEPS = 48
SLOT = 40
ROWS = NSP * SLOT
PAIR = 72
DENSE = NSP * 36
FAR = DENSE // 2
MIXR = 576


def iota(shape, dim):
    return lax.broadcasted_iota(jnp.int32, shape, dim)


def dot(a, b, ca=1, cb=0):
    return lax.dot_general(a, b, (((ca,), (cb,)), ((), ())), preferred_element_type=F32)


def neg_expm1(u):
    poly = u / 40320.0 + 1.0 / 5040.0
    for c in (720.0, 120.0, 24.0, 6.0, 2.0, 1.0):
        poly = poly * u + 1.0 / c
    return -jnp.where(u > -0.5, poly * u, jnp.exp(u) - 1.0)


def silu(x):
    return x * jax.nn.sigmoid(x)


RECV = {}
for _da in range(4):
    for _db in range(4):
        if (_da, _db) != (0, 0):
            for _q in range(2 if _db == 2 or (_da, _db) == (2, 0) else 1):
                RECV[_da, _db, _q] = len(RECV)


class Gather:
    def __init__(self, buf, base, rows, send, recv):
        self.buf, self.base, self.rows, self.send, self.recv = buf, base, rows, send, recv
        t = lax.axis_index("tp")
        self.x, self.y = lax.rem(t, 4), lax.div(t, 4)
        self.sent = []
        self.count = [0, 0]

    def where(self, h, da, db):
        a, b = (self.x, self.y) if h == 0 else (self.y, self.x)
        a, b = lax.rem(a + (da + 8), 4), lax.rem(b + (db + 8), 4)
        return b * 4 + a if h == 0 else a * 4 + b

    def part(self, h, q):
        half, quarter = self.rows // 2, self.rows // 4
        if q is None:
            return pl.ds(self.base + h * half, half)
        return pl.ds(self.base + h * half + q * quarter, quarter)

    def put(self, h, da, db, q, ta, tb):
        at = self.buf.at[self.where(h, -da, -db), self.part(h, q)]
        c = pltpu.make_async_remote_copy(
            src_ref=at,
            dst_ref=at,
            send_sem=self.send.at[h, self.count[h]],
            recv_sem=self.recv.at[h, RECV[(da + ta) % 4, (db + tb) % 4, q or 0]],
            device_id={"tp": self.where(h, ta, tb)},
            device_id_type=MESH,
        )
        self.count[h] += 1
        c.start()
        self.sent.append(c)

    def wait(self, h, da, db, q=None):
        at = self.buf.at[self.where(h, -da, -db), self.part(h, q)]
        pltpu.make_async_remote_copy(
            src_ref=at,
            dst_ref=at,
            send_sem=self.send.at[h, 0],
            recv_sem=self.recv.at[h, RECV[da, db, q or 0]],
            device_id={"tp": self.where(h, 1, 0)},
            device_id_type=MESH,
        ).wait_recv()

    def start(self):
        for h in range(2):
            for ta, tb in ((1, 0), (-1, 0), (0, 1), (0, -1)):
                self.put(h, 0, 0, None, ta, tb)

    def near(self):
        for h in range(2):
            self.wait(h, 1, 0)
            self.put(h, 1, 0, 0, 1, 0)
            self.put(h, 1, 0, None, 0, 1)
            self.put(h, 1, 0, None, 0, -1)
        for h in range(2):
            self.wait(h, 3, 0)
            self.put(h, 3, 0, 1, -1, 0)
            self.put(h, 3, 0, None, 0, 1)
            self.put(h, 3, 0, None, 0, -1)

    def onward(self, h, da):
        self.wait(h, da, 1)
        self.put(h, da, 1, 0, 0, 1)
        self.wait(h, da, 3)
        self.put(h, da, 3, 1, 0, -1)

    def middle(self):
        for h in range(2):
            self.onward(h, 0)
        for h in range(2):
            self.wait(h, 2, 0, 0)
            self.wait(h, 2, 0, 1)
            self.put(h, 2, 0, None, 0, 1)
            self.put(h, 2, 0, None, 0, -1)
        for da in (1, 3):
            for h in range(2):
                self.onward(h, da)

    def rest(self):
        for h in range(2):
            self.onward(h, 2)
        for da in (0, 1, 3, 2):
            for h in range(2):
                for q in range(2):
                    self.wait(h, da, 2, q)

    def drain(self):
        for c in self.sent:
            c.wait_send()


def kernel(
    rec_ref,
    gate_ref,
    conv_ref,
    dw_ref,
    dn_ref,
    iw_ref,
    in_ref,
    base_ref,
    extra_ref,
    tok_ref,
    outw_ref,
    gain_ref,
    sg_ref,
    su_ref,
    sd_ref,
    eg_ref,
    eu_ref,
    ed_ref,
    routes_ref,
    rw_ref,
    out_ref,
    rp,
    hl,
    hr,
    av,
    bv,
    gp,
    tot,
    car,
    mixb,
    wd,
    ww,
    wsgu,
    wegu,
    wsd,
    wed,
    resid,
    sqb,
    nbuf,
    hsbuf,
    rbuf,
    hrbuf,
    outgo,
    arr,
    back,
    ret,
    pt,
    pk0,
    pk1,
    wsem,
    halo_s,
    halo_r,
    car_s,
    car_r,
    sq_s,
    sq_r,
    go_s,
    go_r,
    re_s,
    re_r,
    *gather_sems,
):
    s, t = lax.axis_index("sp"), lax.axis_index("tp")

    barrier = pltpu.get_barrier_semaphore()

    def greet_sp(k, c):
        pl.semaphore_signal(
            barrier, inc=1, device_id={"sp": lax.rem(s + k, NSP)}, device_id_type=MESH
        )
        return c

    def greet_tp(k, c):
        pl.semaphore_signal(
            barrier, inc=1, device_id={"tp": lax.rem(t + k, NTP)}, device_id_type=MESH
        )
        return c

    lax.fori_loop(1, NSP, greet_sp, 0)
    lax.fori_loop(1, NTP, greet_tp, 0)

    r_i, t_i = iota((TOK, TOK), 0), iota((TOK, TOK), 1)
    order = (t_i == (r_i & 7) * STEPS + (r_i >> 3)).astype(BF)
    rp[pl.ds(16, TOK)] = dot(order, rec_ref[...], 1, 1)

    pl.semaphore_wait(barrier, NSP - 1 + NTP - 1)

    up, down = lax.rem(s + 1, NSP), lax.rem(s + NSP - 1, NSP)
    halo_up = pltpu.make_async_remote_copy(
        src_ref=rp.at[pl.ds(16 + 46 * 8, 16)],
        dst_ref=hl,
        send_sem=halo_s.at[0],
        recv_sem=halo_r.at[0],
        device_id={"sp": up},
        device_id_type=MESH,
    )
    halo_up.start()
    halo_down = pltpu.make_async_remote_copy(
        src_ref=rp.at[pl.ds(16, 8)],
        dst_ref=hr,
        send_sem=halo_s.at[1],
        recv_sem=halo_r.at[1],
        device_id={"sp": down},
        device_id_type=MESH,
    )
    halo_down.start()

    loads = []

    def load(src, dst):
        c = pltpu.make_async_copy(src, dst, wsem.at[len(loads)])
        c.start()
        loads.append(c)

    ww[...] = jnp.zeros_like(ww)
    load(outw_ref.at[:, pl.ds(0, WIDE)], wd)
    load(outw_ref.at[:, pl.ds(WIDE, 64)], ww.at[:, pl.ds(0, 64), pl.ds(0, 128)])
    load(outw_ref.at[:, pl.ds(WIDE, 64)], ww.at[:, pl.ds(64, 64), pl.ds(128, 128)])
    n_out = len(loads)
    load(sg_ref, wsgu.at[:, pl.ds(0, 128)])
    load(su_ref, wsgu.at[:, pl.ds(128, 128)])
    load(sd_ref, wsd)
    n_shared = len(loads)
    load(eg_ref, wegu.at[:, pl.ds(0, 128)])
    load(eu_ref, wegu.at[:, pl.ds(128, 128)])
    load(ed_ref, wed)


    for d in range(2):
        rows = jnp.concatenate(
            [
                jnp.broadcast_to(extra_ref[d, 0], (WIDE, TOK)),
                jnp.broadcast_to(extra_ref[d, 1], (CH - WIDE, TOK)),
            ],
            axis=0,
        )
        high = rows.astype(BF)
        left = rows - high.astype(F32)
        mid = left.astype(BF)
        low = (left - mid.astype(F32)).astype(BF)
        av[d] = (dot(order, high, 1, 1) + dot(order, mid, 1, 1)) + dot(order, low, 1, 1)

    halo_up.wait_recv()
    halo_down.wait_recv()
    sub = iota((8, CH), 0)
    first, last = s == 0, s == NSP - 1
    for k in range(2):
        edge = jnp.where(first, 0.0, hl[pl.ds(k * 8 + 7, 1)])
        rolled = pltpu.roll(rp[pl.ds(16 + (46 + k) * 8, 8)], 1, 0)
        rp[pl.ds(k * 8, 8)] = jnp.where(sub == 0, edge, rolled)
    edge = jnp.where(last, 0.0, hr[pl.ds(0, 1)])
    rolled = pltpu.roll(rp[pl.ds(16, 8)], 7, 0)
    rp[pl.ds(16 + TOK, 8)] = jnp.where(sub == 7, edge, rolled)
    taps = conv_ref[...].astype(F32)

    block = 64
    for i in range(TOK // block):
        r0 = i * block
        conv = rp[pl.ds(r0, block)] * taps[0:1]
        for j in range(1, 4):
            conv = conv + rp[pl.ds(r0 + 8 * j, block)] * taps[j : j + 1]
        conv_b = conv.astype(BF)
        conv_f = conv_b.astype(F32)
        wide, narrow = conv_b[:, :WIDE], conv_b[:, WIDE:]
        for d in range(2):
            rate = jax.nn.sigmoid(
                jnp.concatenate([dot(wide, dw_ref[d]), dot(narrow, dn_ref[d])], axis=1)
            )
            admit = jax.nn.sigmoid(
                jnp.concatenate([dot(wide, iw_ref[d]), dot(narrow, in_ref[d])], axis=1)
            )
            log_decay = -RATE_SCALE * rate * base_ref[d : d + 1] + av[d, pl.ds(r0, block)]
            drive = jnp.sqrt(neg_expm1(2.0 * log_decay)) * admit * conv_f
            av[d, pl.ds(r0, block)] = jnp.exp(log_decay)
            bv[d, pl.ds(r0, block)] = drive

    def scan(i, carry):
        c0, s0, c1, s1 = carry
        f = pl.ds(pl.multiple_of(i * 8, 8), 8)
        g = pl.ds(pl.multiple_of((STEPS - 1 - i) * 8, 8), 8)
        a0, a1 = av[0, f], av[1, g]
        s0, s1 = a0 * s0 + bv[0, f], a1 * s1 + bv[1, g]
        c0, c1 = a0 * c0, a1 * c1
        av[0, f], av[1, g] = c0, c1
        bv[0, f], bv[1, g] = s0, s1
        return c0, s0, c1, s1

    one, zero = jnp.ones((8, CH), F32), jnp.zeros((8, CH), F32)
    c0, s0, c1, s1 = lax.fori_loop(0, STEPS, scan, (one, zero, one, zero), unroll=4)

    def chunks(c, st, sequence):
        g, h = jnp.ones((1, CH), F32), jnp.zeros((1, CH), F32)
        gin, hin = zero, zero
        for k in sequence:
            gin = jnp.where(sub == k, g, gin)
            hin = jnp.where(sub == k, h, hin)
            ck, sk = c[k : k + 1], st[k : k + 1]
            g, h = ck * g, ck * h + sk
        return gin, hin, g, h

    g0, h0, gt0, ht0 = chunks(c0, s0, range(8))
    g1, h1, gt1, ht1 = chunks(c1, s1, range(7, -1, -1))
    tot[0, pl.ds(0, 1)] = gt0
    tot[0, pl.ds(1, 1)] = ht0
    tot[1, pl.ds(0, 1)] = gt1
    tot[1, pl.ds(1, 1)] = ht1

    def carry_copy(k):
        dest = lax.rem(s + k, NSP)
        return pltpu.make_async_remote_copy(
            src_ref=tot.at[(dest < s).astype(jnp.int32)],
            dst_ref=car.at[s],
            send_sem=car_s.at[k],
            recv_sem=car_r.at[s],
            device_id={"sp": dest},
            device_id_type=MESH,
        )

    def carry_start(k, c):
        carry_copy(k).start()
        return c

    lax.fori_loop(1, NSP, carry_start, 0)
    car[s] = jnp.zeros((2, CH), F32)

    gp[...] = jax.nn.gelu(dot(order, gate_ref[...], 1, 1))
    routes = routes_ref[...].astype(F32)
    e0, e1 = routes[0:1], routes[1:2]
    e_i = iota((NSP, TOK), 0).astype(F32)
    hit0, hit1 = e_i == e0, e_i == e1
    named = jnp.where(hit0, 1.0, 0.0) + jnp.where(hit1, 1.0, 0.0)
    rank = dot(named.astype(BF), (r_i < t_i).astype(BF))
    def rel(e):
        k = e - (s - 8).astype(F32)
        k = jnp.where(k < 0.0, k + NSP, k)
        return jnp.where(k >= NSP, k - NSP, k)

    place0 = rel(e0) * SLOT + jnp.sum(jnp.where(hit0, rank, 0.0), axis=0, keepdims=True)
    place1 = rel(e1) * SLOT + jnp.sum(jnp.where(hit1, rank, 0.0), axis=0, keepdims=True)
    for k in range(ROWS // 128):
        s_i = (iota((128, TOK), 0) + k * 128).astype(F32)
        pt[pl.ds(k * 128, 128)] = (
            jnp.where(s_i == place0, 1.0, 0.0) + jnp.where(s_i == place1, 1.0, 0.0)
        ).astype(BF)
    col0 = jnp.transpose(jnp.broadcast_to(place0, (128, TOK)))
    col1 = jnp.transpose(jnp.broadcast_to(place1, (128, TOK)))
    for k in range(ROWS // 128):
        l_i = (iota((TOK, 128), 1) + k * 128).astype(F32)
        pk0[:, pl.ds(k * 128, 128)] = jnp.where(l_i == col0, 1.0, 0.0).astype(BF)
        pk1[:, pl.ds(k * 128, 128)] = jnp.where(l_i == col1, 1.0, 0.0).astype(BF)


    def carry_wait(k, c):
        src = lax.rem(s + k, NSP)
        pltpu.make_async_remote_copy(
            src_ref=tot.at[0],
            dst_ref=car.at[src],
            send_sem=car_s.at[k],
            recv_sem=car_r.at[src],
            device_id={"sp": src},
            device_id_type=MESH,
        ).wait_recv()
        return c

    lax.fori_loop(1, NSP, carry_wait, 0)
    ahead, behind = jnp.zeros((1, CH), F32), jnp.zeros((1, CH), F32)
    for j in range(NSP):
        cj = car[j]
        ahead = jnp.where(j < s, cj[0:1] * ahead + cj[1:2], ahead)
        cj = car[NSP - 1 - j]
        behind = jnp.where(NSP - 1 - j > s, cj[0:1] * behind + cj[1:2], behind)
    x0, x1 = h0 + g0 * ahead, h1 + g1 * behind

    for i in range(STEPS):
        f = pl.ds(i * 8, 8)
        total = (bv[0, f] + av[0, f] * x0) + (bv[1, f] + av[1, f] * x1)
        bv[0, f] = total * gp[f]
    tok_i, row_i = iota((TOK, TOK), 0), iota((TOK, TOK), 1)
    chunk = sum(jnp.where(tok_i >= STEPS * k, 1, 0) for k in range(1, 8))
    back_order = (row_i == (tok_i - chunk * STEPS) * 8 + chunk).astype(BF)
    mixed = dot(back_order, bv[0].astype(BF)).astype(BF)
    c_i, l_i = iota((CH, 128), 0), iota((CH, 128), 1)
    low = ((c_i == l_i + WIDE) & (l_i < 64)).astype(BF)
    high = ((c_i == l_i + 64) & (l_i >= 64)).astype(BF)
    gathers = [
        Gather(buf, base, rows, *gather_sems[2 * k : 2 * k + 2])
        for k, (buf, base, rows) in enumerate(
            (
                (mixb, 0, MIXR),
                (nbuf, 0, TOK),
                (hsbuf, 0, TOK),
                (rbuf, 0, FAR),
                (rbuf, FAR, FAR),
                (hrbuf, 0, FAR),
                (hrbuf, FAR, FAR),
            )
        )
    ]
    gm, gn, gs, r0, r1, f0, f1 = gathers
    mixb[t, pl.ds(0, TOK)] = mixed[:, :WIDE]
    mixb[t, pl.ds(TOK, 192)] = (dot(mixed[:192], low) + dot(mixed[192:], high)).astype(BF)
    gm.start()
    gm.near()
    gm.middle()
    gm.rest()
    for c in loads[:n_out]:
        c.wait()

    lhs = jnp.concatenate([mixb[j, pl.ds(0, TOK)] for j in range(NTP)], axis=1)
    res = tok_ref[...].astype(F32) + dot(lhs, wd[...].reshape(NTP * WIDE, 128))
    lhs = jnp.concatenate([mixb[j, pl.ds(TOK, 192)] for j in range(NTP)], axis=1)
    add = dot(lhs, ww[...].reshape(NTP * WIDE, 256))
    res = res + jnp.concatenate([add[:, :128], add[:, 128:]], axis=0)
    resid[...] = res
    nbuf[t] = (res * gain_ref[...]).astype(BF)
    gn.start()

    sqb[t] = jnp.sum(jnp.transpose(res * res), axis=0, keepdims=True)

    def sq_start(k, c):
        pltpu.make_async_remote_copy(
            src_ref=sqb.at[t],
            dst_ref=sqb.at[t],
            send_sem=sq_s.at[k],
            recv_sem=sq_r.at[t],
            device_id={"tp": lax.rem(t + k, NTP)},
            device_id_type=MESH,
        ).start()
        return c

    def sq_wait(k, c):
        src = lax.rem(t + k, NTP)
        pltpu.make_async_remote_copy(
            src_ref=sqb.at[t],
            dst_ref=sqb.at[src],
            send_sem=sq_s.at[k],
            recv_sem=sq_r.at[src],
            device_id={"tp": src},
            device_id_type=MESH,
        ).wait_recv()
        return c

    lax.fori_loop(1, NTP, sq_start, 0)
    gn.near()
    lax.fori_loop(1, NTP, sq_wait, 0)
    square = sqb[0]
    for j in range(1, NTP):
        square = square + sqb[j]
    scale = lax.rsqrt(square / D + NORM_EPS)
    scale = jnp.transpose(jnp.broadcast_to(scale, (128, TOK)))
    normed = (resid[...] * scale * gain_ref[...]).astype(BF)

    outgo[...] = dot(pt[...], normed).astype(BF)

    def place(k):
        return pl.ds(pl.multiple_of(lax.rem(k + 2 * NSP, NSP) * SLOT, 8), SLOT)

    def go_start(k, c):
        dest = lax.rem(s + k, NSP)
        pltpu.make_async_remote_copy(
            src_ref=outgo.at[place(k + 8)],
            dst_ref=arr.at[place(8 - k)],
            send_sem=go_s.at[k],
            recv_sem=go_r.at[lax.rem(NSP - k, NSP)],
            device_id={"sp": dest},
            device_id_type=MESH,
        ).start()
        return c

    def go_wait(k):
        pltpu.make_async_remote_copy(
            src_ref=outgo.at[place(0)],
            dst_ref=arr.at[place(k + 8)],
            send_sem=go_s.at[k],
            recv_sem=go_r.at[k],
            device_id={"sp": lax.rem(s + k, NSP)},
            device_id_type=MESH,
        ).wait_recv()

    def both_ways(a, b, op):
        def step(k, c):
            op(k, c)
            op(NSP - k, c)
            return c

        lax.fori_loop(a, b, step, 0)

    both_ways(1, 16, go_start)
    go_start(16, 0)
    arr[pl.ds(8 * SLOT, SLOT)] = outgo[pl.ds(8 * SLOT, SLOT)]

    p_i, q_i = iota((PAIR, 2 * SLOT), 0), iota((PAIR, 2 * SLOT), 1)
    skip = jnp.where(p_i >= 36, SLOT - 36, 0)
    squeeze = (q_i == p_i + skip).astype(BF)
    p_i, q_i = iota((2 * SLOT, PAIR), 0), iota((2 * SLOT, PAIR), 1)
    spread = ((p_i == q_i + jnp.where(q_i >= 36, SLOT - 36, 0))).astype(BF)

    def pack(c):
        for k in range(8):
            rows = arr[pl.ds((c * 8 + k) * 2 * SLOT, 2 * SLOT)]
            rbuf[t, pl.ds((c * 8 + k) * PAIR, PAIR)] = dot(squeeze, rows).astype(BF)

    def near_wait(k, c):
        go_wait(k)
        return c

    gn.middle()
    gn.rest()
    for c in loads[n_out:n_shared]:
        c.wait()
    lhs = jnp.concatenate([nbuf[j] for j in range(NTP)], axis=1)
    both = dot(lhs, wsgu[...])
    hsbuf[t] = (silu(both[:, :128] * scale) * (both[:, 128:] * scale)).astype(BF)
    gs.start()
    lax.fori_loop(1, 8, near_wait, 0)
    lax.fori_loop(24, NSP, near_wait, 0)
    pack(0)
    r0.start()
    gs.near()
    r0.near()
    gs.middle()
    lax.fori_loop(8, 24, near_wait, 0)
    pack(1)
    r1.start()
    r0.middle()
    gs.rest()
    r1.near()
    r0.rest()
    for c in loads[n_shared:]:
        c.wait()

    def routed(c):
        def step(i, carry):
            r = pl.ds(pl.multiple_of(c * FAR + i * 192, 8), 192)
            left = jnp.concatenate([rbuf[j, r] for j in range(NTP)], axis=1)
            both = dot(left, wegu[...])
            hrbuf[t, r] = (silu(both[:, :128]) * both[:, 128:]).astype(BF)
            return carry

        lax.fori_loop(0, FAR // 192, step, 0)

    routed(0)
    r1.middle()
    f0.start()
    r1.rest()
    routed(1)
    f1.start()
    f1.near()
    f0.near()
    f1.middle()
    lhs = jnp.concatenate([hsbuf[j] for j in range(NTP)], axis=1)
    resid[...] += dot(lhs, wsd[...])
    f1.rest()

    def re_start(k, c):
        pltpu.make_async_remote_copy(
            src_ref=back.at[place(k + 8)],
            dst_ref=ret.at[place(8 - k)],
            send_sem=re_s.at[k],
            recv_sem=re_r.at[lax.rem(NSP - k, NSP)],
            device_id={"sp": lax.rem(s + k, NSP)},
            device_id_type=MESH,
        ).start()
        return c

    def re_wait(k, c):
        pltpu.make_async_remote_copy(
            src_ref=back.at[place(0)],
            dst_ref=ret.at[place(k + 8)],
            send_sem=re_s.at[k],
            recv_sem=re_r.at[k],
            device_id={"sp": lax.rem(s + k, NSP)},
            device_id_type=MESH,
        ).wait_recv()
        return c

    def down(c):
        left = jnp.concatenate([hrbuf[j, pl.ds(c * FAR, FAR)] for j in range(NTP)], axis=1)
        y = dot(left, wed[...]).astype(BF)
        for k in range(8):
            back[pl.ds((c * 8 + k) * 2 * SLOT, 2 * SLOT)] = dot(
                spread, y[k * PAIR : (k + 1) * PAIR]
            ).astype(BF)

    down(1)
    re_start(16, 0)
    both_ways(9, 16, re_start)
    re_start(8, 0)
    f0.middle()
    f0.rest()
    down(0)
    re_start(24, 0)
    both_ways(1, 8, re_start)
    ret[pl.ds(8 * SLOT, SLOT)] = back[pl.ds(8 * SLOT, SLOT)]

    halo_up.wait_send()
    halo_down.wait_send()
    for g in gathers:
        g.drain()

    def drain_sp(k, c):
        carry_copy(k).wait_send()
        for sem in (go_s, re_s):
            pltpu.make_async_remote_copy(
                src_ref=outgo.at[pl.ds(0, SLOT)],
                dst_ref=ret.at[pl.ds(0, SLOT)],
                send_sem=sem.at[k],
                recv_sem=re_r.at[s],
                device_id={"sp": lax.rem(s + k, NSP)},
                device_id_type=MESH,
            ).wait_send()
        return c

    def drain_tp(k, c):
        pltpu.make_async_remote_copy(
            src_ref=sqb.at[t],
            dst_ref=sqb.at[t],
            send_sem=sq_s.at[k],
            recv_sem=sq_r.at[t],
            device_id={"tp": lax.rem(t + k, NTP)},
            device_id_type=MESH,
        ).wait_send()
        return c

    weights = rw_ref[...]
    w0 = jnp.transpose(jnp.broadcast_to(weights[0:1], (128, TOK)))
    w1 = jnp.transpose(jnp.broadcast_to(weights[1:2], (128, TOK)))
    lax.fori_loop(1, NTP, drain_tp, 0)
    half = ROWS // 2

    def combine(c):
        at = pl.ds(c * half, half)
        got = ret[at]
        return w0 * dot(pk0[:, at], got) + w1 * dot(pk1[:, at], got)

    lax.fori_loop(8, 24, re_wait, 0)
    resid[...] += combine(1)
    lax.fori_loop(1, 8, re_wait, 0)
    lax.fori_loop(24, NSP, re_wait, 0)
    out_ref[...] = (resid[...] + combine(0)).astype(BF)
    lax.fori_loop(1, NSP, drain_sp, 0)


def layer(
    rec_input,
    gate_input,
    conv_weight,
    decay_wide,
    decay_narrow,
    input_wide,
    input_narrow,
    decay_base,
    decay_extra,
    tokens,
    out_weight,
    norm_gain,
    shared_gate,
    shared_up,
    shared_down,
    expert_gate,
    expert_up,
    expert_down,
    routes,
    route_weight,
):
    vmem = pl.BlockSpec(memory_space=pltpu.VMEM)
    hbm = pl.BlockSpec(memory_space=pl.ANY)
    dma = pltpu.SemaphoreType.DMA
    gather_sems = [dma((2, 20)), dma((2, len(RECV)))] * 7
    return pl.pallas_call(
        kernel,
        out_shape=jax.ShapeDtypeStruct((TOK, 128), BF),
        in_specs=[vmem] * 10 + [hbm] + [vmem] + [hbm] * 6 + [vmem] * 2,
        out_specs=vmem,
        scratch_shapes=[
            pltpu.VMEM((TOK + 24, CH), F32),
            pltpu.VMEM((16, CH), F32),
            pltpu.VMEM((8, CH), F32),
            pltpu.VMEM((2, TOK, CH), F32),
            pltpu.VMEM((2, TOK, CH), F32),
            pltpu.VMEM((TOK, CH), F32),
            pltpu.VMEM((2, 2, CH), F32),
            pltpu.VMEM((NSP, 2, CH), F32),
            pltpu.VMEM((NTP, 2 * MIXR, 128), BF),
            pltpu.VMEM((NTP, WIDE, 128), BF),
            pltpu.VMEM((NTP, WIDE, 256), BF),
            pltpu.VMEM((D, 256), BF),
            pltpu.VMEM((D, 256), BF),
            pltpu.VMEM((D, 128), BF),
            pltpu.VMEM((D, 128), BF),
            pltpu.VMEM((TOK, 128), F32),
            pltpu.VMEM((NTP, 1, TOK), F32),
            pltpu.VMEM((NTP, TOK, 128), BF),
            pltpu.VMEM((NTP, TOK, 128), BF),
            pltpu.VMEM((NTP, DENSE, 128), BF),
            pltpu.VMEM((NTP, DENSE, 128), BF),
            pltpu.VMEM((ROWS, 128), BF),
            pltpu.VMEM((ROWS, 128), BF),
            pltpu.VMEM((ROWS, 128), BF),
            pltpu.VMEM((ROWS, 128), BF),
            pltpu.VMEM((ROWS, TOK), BF),
            pltpu.VMEM((TOK, ROWS), BF),
            pltpu.VMEM((TOK, ROWS), BF),
            dma((9,)),
            dma((2,)),
            dma((2,)),
            dma((NSP,)),
            dma((NSP,)),
            dma((NTP,)),
            dma((NTP,)),
            dma((NSP,)),
            dma((NSP,)),
            dma((NSP,)),
            dma((NSP,)),
            *gather_sems,
        ],
        compiler_params=pltpu.CompilerParams(
            collective_id=0, has_side_effects=True, vmem_limit_bytes=60 * 1024 * 1024
        ),
        name="layer",
    )(
        rec_input.T,
        gate_input.T,
        conv_weight,
        decay_wide[:, 0],
        decay_narrow[:, 0],
        input_wide[:, 0],
        input_narrow[:, 0],
        decay_base,
        decay_extra.transpose(0, 2, 3, 1),
        tokens,
        out_weight.reshape(NTP, CH, 128),
        norm_gain.reshape(1, 128),
        shared_gate,
        shared_up,
        shared_down,
        expert_gate[0],
        expert_up[0],
        expert_down[0],
        routes.T,
        route_weight.T,
    )


def solution(mesh):
    return jax.shard_map(
        layer,
        mesh=mesh,
        in_specs=(
            P("sp", "tp"),
            P("sp", "tp"),
            P(None, "tp"),
            P(None, "tp", None, None),
            P(None, "tp", None, None),
            P(None, "tp", None, None),
            P(None, "tp", None, None),
            P(None, "tp"),
            P(None, "sp", None, "tp"),
            P("sp", "tp"),
            P(None, "tp"),
            P("tp"),
            P(None, "tp"),
            P(None, "tp"),
            P(None, "tp"),
            P("sp", None, "tp"),
            P("sp", None, "tp"),
            P("sp", None, "tp"),
            P("sp", None),
            P("sp", None),
        ),
        out_specs=P("sp", "tp"),
        check_vma=False,
    )
```

profile of v0, /device:TPU:1, one launch (start us, length us, event | category | flops | bytes accessed | tf_op | source)
XLA Modules:
  0.0 157.1 jit_solution(2035666322568589955)
XLA Ops:
  0.0 155.5 %layer.1 = bf16[384,128]{1,0:T(8,128)(2,1)} custom-call(bf16[192,384]{1,0:T(8,128)(2,1)} %bitcast.18, bf16[192,384]{1,0:T(8,128)(2,1)} %bitcast.19, bf16[4,192]{1,0:T(4,128)(2,1)} %conv_ref.1, bf16[2,128,128]{2,1,0:T(8,128)(2,1)} %bitcast.20, bf16[2,64,64]{2,1,0:T(8,128)(2,1)} %bitcast.22, bf16[2,128,128]{2,1,0:T(8,128)(2,1)} %bitcast.21, ...), custom_call_target="tpu_custom_call" | custom-call | tf_op jit(solution)/shard_map/layer/pallas_call | solution.py:719
  155.5 1.5 copy.22
where the time goes:
time: 157 us
  Pallas kernels  156 us (99%)
    pallas_call x1, Pallas kernels, layer(): pl.pallas_call(kernel, out_shape=jax.ShapeDtypeStruct((TOK, 128), BF), in...  156 us

commit v1 on v0

--- a/solution.py
+++ b/solution.py
@@ -24,6 +24,7 @@
 PAIR = 72
 DENSE = NSP * 36
 FAR = DENSE // 2
+CHUNK = DENSE // 4
 MIXR = 576
 
 
@@ -44,6 +45,66 @@
 
 def silu(x):
     return x * jax.nn.sigmoid(x)
+
+
+MIX_ORDER = (
+    (0, 0, 0, 1, 0), (0, 0, 0, 3, 0), (0, 0, 1, 0, 0), (0, 0, 3, 0, 0), (0, 1, 0, 1, 0),
+    (0, 1, 0, 3, 0), (0, 1, 1, 0, 0), (0, 1, 3, 0, 0), (0, 0, 2, 0, 0), (0, 0, 2, 0, 1),
+    (0, 0, 1, 1, 0), (0, 0, 1, 3, 0), (0, 0, 3, 1, 0), (0, 1, 1, 1, 0), (0, 0, 3, 3, 0),
+    (0, 1, 1, 3, 0), (0, 1, 2, 0, 0), (0, 1, 2, 0, 1), (0, 1, 3, 1, 0), (0, 1, 3, 3, 0),
+    (0, 0, 2, 1, 0), (0, 0, 2, 3, 0), (0, 1, 2, 1, 0), (0, 1, 2, 3, 0),
+)
+ORDER = (
+    (0, 0, 0, 1, 0), (0, 0, 0, 3, 0), (0, 0, 1, 0, 0), (0, 0, 3, 0, 0), (0, 1, 0, 1, 0),
+    (0, 1, 0, 3, 0), (0, 1, 1, 0, 0), (0, 1, 3, 0, 0), (0, 0, 2, 0, 0), (0, 0, 2, 0, 1),
+    (0, 0, 1, 1, 0), (0, 0, 1, 3, 0), (0, 0, 3, 1, 0), (0, 1, 1, 1, 0), (0, 0, 3, 3, 0),
+    (0, 1, 1, 3, 0), (0, 1, 2, 0, 0), (0, 1, 2, 0, 1), (0, 1, 3, 1, 0), (0, 1, 3, 3, 0),
+    (0, 0, 2, 1, 0), (0, 0, 2, 3, 0), (0, 1, 2, 1, 0), (0, 1, 2, 3, 0), "pack3", "shared",
+    (5, 0, 0, 1, 0), (5, 0, 0, 3, 0), (5, 0, 1, 0, 0), (5, 0, 3, 0, 0), (5, 1, 0, 1, 0),
+    (5, 1, 0, 3, 0), (5, 1, 1, 0, 0), (5, 1, 3, 0, 0), (1, 0, 0, 1, 0), (1, 0, 0, 3, 0),
+    (1, 0, 1, 0, 0), (1, 0, 3, 0, 0), "pack2", (1, 1, 0, 1, 0), (1, 1, 0, 3, 0), (1, 1, 1, 0, 0),
+    (1, 1, 3, 0, 0), (5, 0, 2, 0, 0), (5, 0, 2, 0, 1), (5, 0, 1, 1, 0), (5, 0, 1, 3, 0), "pack1",
+    (5, 1, 1, 1, 0), (5, 0, 3, 1, 0), (5, 0, 3, 3, 0), (5, 1, 1, 3, 0), (5, 1, 2, 0, 0),
+    (5, 1, 2, 0, 1), (5, 1, 3, 1, 0), (5, 1, 3, 3, 0), "pack0", (1, 0, 2, 0, 0), (1, 0, 2, 0, 1),
+    "sq2", (1, 0, 1, 1, 0), (1, 0, 1, 3, 0), (4, 0, 1, 0, 0), (4, 0, 3, 0, 0), (4, 1, 0, 1, 0),
+    (4, 1, 0, 3, 0), (1, 0, 3, 1, 0), (1, 0, 3, 3, 0), (4, 0, 0, 1, 0), (4, 0, 0, 3, 0),
+    (1, 1, 1, 1, 0), (1, 1, 1, 3, 0), (4, 1, 1, 0, 0), (4, 1, 3, 0, 0), (1, 1, 2, 0, 0),
+    (1, 1, 2, 0, 1), (1, 1, 3, 1, 0), (1, 1, 3, 3, 0), (5, 0, 2, 1, 0), (5, 0, 2, 3, 0),
+    (3, 0, 1, 0, 0), (3, 0, 3, 0, 0), (3, 1, 0, 1, 0), (3, 0, 0, 1, 0), (3, 0, 0, 3, 0),
+    (3, 1, 0, 3, 0), (3, 1, 1, 0, 0), (3, 1, 3, 0, 0), (5, 1, 2, 1, 0), (5, 1, 2, 3, 0),
+    (2, 0, 0, 1, 0), (2, 0, 0, 3, 0), (2, 0, 1, 0, 0), (2, 0, 3, 0, 0), (2, 1, 1, 0, 0),
+    (2, 1, 3, 0, 0), (2, 1, 0, 1, 0), (2, 1, 0, 3, 0), (4, 0, 2, 0, 0), (4, 0, 2, 0, 1),
+    (1, 0, 2, 1, 0), (1, 0, 2, 3, 0), (4, 0, 1, 1, 0), (4, 0, 1, 3, 0), (4, 1, 1, 1, 0),
+    (4, 1, 1, 3, 0), (4, 0, 3, 1, 0), (4, 0, 3, 3, 0), (4, 1, 3, 1, 0), (4, 1, 3, 3, 0),
+    (1, 1, 2, 1, 0), (1, 1, 2, 3, 0), (4, 1, 2, 0, 0), (4, 1, 2, 0, 1), (3, 0, 2, 0, 0),
+    (3, 0, 2, 0, 1), (3, 0, 1, 1, 0), (3, 0, 1, 3, 0), (3, 1, 1, 1, 0), (3, 0, 3, 1, 0),
+    (3, 0, 3, 3, 0), (3, 1, 1, 3, 0), (3, 1, 3, 1, 0), (3, 1, 2, 0, 0), (3, 1, 2, 0, 1),
+    (3, 1, 3, 3, 0), "routed3", (2, 0, 2, 0, 0), (2, 0, 2, 0, 1), (2, 0, 1, 1, 0), (2, 0, 1, 3, 0),
+    (2, 1, 1, 1, 0), (2, 1, 1, 3, 0), (2, 0, 3, 1, 0), (2, 0, 3, 3, 0), (2, 1, 3, 1, 0),
+    (2, 1, 2, 0, 0), (2, 1, 2, 0, 1), (2, 1, 3, 3, 0), (4, 0, 2, 1, 0), (4, 0, 2, 3, 0), "sdown",
+    (4, 1, 2, 1, 0), (4, 1, 2, 3, 0), (3, 0, 2, 1, 0), (3, 0, 2, 3, 0), (3, 1, 2, 3, 0),
+    (3, 1, 2, 1, 0), (9, 0, 0, 1, 0), (9, 0, 0, 3, 0), (9, 0, 1, 0, 0), (9, 0, 3, 0, 0),
+    (9, 1, 1, 0, 0), (9, 1, 3, 0, 0), (9, 1, 0, 1, 0), (9, 1, 0, 3, 0), (2, 0, 2, 1, 0),
+    (2, 0, 2, 3, 0), (2, 1, 2, 3, 0), (2, 1, 2, 1, 0), "routed2", (9, 0, 2, 0, 0), (9, 0, 2, 0, 1),
+    "routed1", (9, 0, 1, 1, 0), (9, 0, 1, 3, 0), (9, 1, 1, 1, 0), (9, 1, 1, 3, 0), (9, 0, 3, 1, 0),
+    (9, 0, 3, 3, 0), (9, 1, 3, 1, 0), (9, 1, 2, 0, 0), (9, 1, 2, 0, 1), (9, 1, 3, 3, 0), "routed0",
+    (8, 0, 0, 1, 0), (8, 0, 0, 3, 0), (8, 0, 1, 0, 0), (8, 0, 3, 0, 0), (8, 1, 0, 1, 0),
+    (8, 1, 0, 3, 0), (8, 1, 1, 0, 0), (8, 1, 3, 0, 0), (7, 0, 1, 0, 0), (7, 0, 3, 0, 0),
+    (9, 0, 2, 1, 0), (9, 0, 2, 3, 0), (7, 0, 0, 1, 0), (7, 0, 0, 3, 0), (7, 1, 0, 1, 0),
+    (7, 1, 0, 3, 0), (7, 1, 1, 0, 0), (7, 1, 3, 0, 0), (9, 1, 2, 3, 0), (9, 1, 2, 1, 0),
+    (6, 0, 0, 1, 0), (6, 0, 0, 3, 0), (6, 0, 1, 0, 0), (6, 0, 3, 0, 0), (6, 1, 0, 1, 0),
+    (6, 1, 0, 3, 0), (6, 1, 1, 0, 0), (6, 1, 3, 0, 0), (8, 0, 2, 0, 0), (8, 0, 2, 0, 1),
+    (8, 0, 1, 1, 0), (8, 0, 1, 3, 0), (8, 1, 1, 1, 0), (8, 1, 1, 3, 0), (8, 0, 3, 1, 0),
+    (8, 0, 3, 3, 0), (8, 1, 2, 0, 0), (8, 1, 2, 0, 1), (8, 1, 3, 1, 0), (8, 1, 3, 3, 0),
+    (7, 0, 2, 0, 0), (7, 0, 2, 0, 1), (7, 0, 1, 1, 0), (7, 0, 1, 3, 0), (7, 0, 3, 1, 0),
+    (7, 0, 3, 3, 0), (7, 1, 1, 1, 0), (7, 1, 1, 3, 0), (7, 1, 3, 1, 0), (7, 1, 3, 3, 0),
+    (7, 1, 2, 0, 0), (7, 1, 2, 0, 1), "down3", (6, 0, 2, 0, 0), (6, 0, 2, 0, 1), (6, 0, 1, 1, 0),
+    (6, 0, 1, 3, 0), (6, 1, 1, 1, 0), (6, 1, 1, 3, 0), (6, 0, 3, 1, 0), (6, 0, 3, 3, 0),
+    (6, 1, 2, 0, 0), (6, 1, 2, 0, 1), (6, 1, 3, 1, 0), (6, 1, 3, 3, 0), (8, 0, 2, 1, 0),
+    (8, 0, 2, 3, 0), (8, 1, 2, 1, 0), (8, 1, 2, 3, 0), (7, 0, 2, 1, 0), (7, 0, 2, 3, 0),
+    (7, 1, 2, 1, 0), (7, 1, 2, 3, 0), (6, 0, 2, 1, 0), (6, 0, 2, 3, 0), (6, 1, 2, 1, 0),
+    (6, 1, 2, 3, 0), "down2", "down1", "down0",
+)
 
 
 RECV = {}
@@ -61,6 +122,7 @@
         self.x, self.y = lax.rem(t, 4), lax.div(t, 4)
         self.sent = []
         self.count = [0, 0]
+        self.seen = [0, 0]
 
     def where(self, h, da, db):
         a, b = (self.x, self.y) if h == 0 else (self.y, self.x)
@@ -87,8 +149,9 @@
         c.start()
         self.sent.append(c)
 
-    def wait(self, h, da, db, q=None):
-        at = self.buf.at[self.where(h, -da, -db), self.part(h, q)]
+    def wait(self, h, da, db, q):
+        split = db == 2 or (da, db) == (2, 0)
+        at = self.buf.at[self.where(h, -da, -db), self.part(h, q if split else None)]
         pltpu.make_async_remote_copy(
             src_ref=at,
             dst_ref=at,
@@ -103,39 +166,19 @@
             for ta, tb in ((1, 0), (-1, 0), (0, 1), (0, -1)):
                 self.put(h, 0, 0, None, ta, tb)
 
-    def near(self):
-        for h in range(2):
-            self.wait(h, 1, 0)
-            self.put(h, 1, 0, 0, 1, 0)
-            self.put(h, 1, 0, None, 0, 1)
-            self.put(h, 1, 0, None, 0, -1)
-        for h in range(2):
-            self.wait(h, 3, 0)
-            self.put(h, 3, 0, 1, -1, 0)
-            self.put(h, 3, 0, None, 0, 1)
-            self.put(h, 3, 0, None, 0, -1)
-
-    def onward(self, h, da):
-        self.wait(h, da, 1)
-        self.put(h, da, 1, 0, 0, 1)
-        self.wait(h, da, 3)
-        self.put(h, da, 3, 1, 0, -1)
-
-    def middle(self):
-        for h in range(2):
-            self.onward(h, 0)
-        for h in range(2):
-            self.wait(h, 2, 0, 0)
-            self.wait(h, 2, 0, 1)
-            self.put(h, 2, 0, None, 0, 1)
-            self.put(h, 2, 0, None, 0, -1)
-        for da in (1, 3):
-            for h in range(2):
-                self.onward(h, da)
-
-    def rest(self):
-        for h in range(2):
-            self.onward(h, 2)
+    def take(self, h, da, db, q):
+        self.wait(h, da, db, q)
+        if db == 0 and da != 2:
+            self.put(h, da, 0, 0 if da == 1 else 1, 2 - da, 0)
+        if db == 0:
+            self.seen[h] += da == 2
+            if da != 2 or self.seen[h] == 2:
+                self.put(h, da, 0, None, 0, 1)
+                self.put(h, da, 0, None, 0, -1)
+        else:
+            self.put(h, da, db, 0 if db == 1 else 1, 0, 2 - db)
+
+    def finish(self):
         for da in (0, 1, 3, 2):
             for h in range(2):
                 for q in range(2):
@@ -185,6 +228,8 @@
     wed,
     resid,
     sqb,
+    sq2b,
+    sc2,
     nbuf,
     hsbuf,
     rbuf,
@@ -203,6 +248,8 @@
     car_r,
     sq_s,
     sq_r,
+    sq2_s,
+    sq2_r,
     go_s,
     go_r,
     re_s,
@@ -380,9 +427,9 @@
     named = jnp.where(hit0, 1.0, 0.0) + jnp.where(hit1, 1.0, 0.0)
     rank = dot(named.astype(BF), (r_i < t_i).astype(BF))
     def rel(e):
-        k = e - (s - 8).astype(F32)
+        k = e - s.astype(F32)
         k = jnp.where(k < 0.0, k + NSP, k)
-        return jnp.where(k >= NSP, k - NSP, k)
+        return jnp.where(k > 16.0, 64.0 - 2.0 * k, jnp.maximum(2.0 * k - 1.0, 0.0))
 
     place0 = rel(e0) * SLOT + jnp.sum(jnp.where(hit0, rank, 0.0), axis=0, keepdims=True)
     place1 = rel(e1) * SLOT + jnp.sum(jnp.where(hit1, rank, 0.0), axis=0, keepdims=True)
@@ -438,20 +485,18 @@
                 (mixb, 0, MIXR),
                 (nbuf, 0, TOK),
                 (hsbuf, 0, TOK),
-                (rbuf, 0, FAR),
-                (rbuf, FAR, FAR),
-                (hrbuf, 0, FAR),
-                (hrbuf, FAR, FAR),
+                *((b, c * CHUNK, CHUNK) for b in (rbuf, hrbuf) for c in range(4)),
             )
         )
     ]
-    gm, gn, gs, r0, r1, f0, f1 = gathers
+    gm, gn, gs = gathers[:3]
+    gr, gf = gathers[3:7], gathers[7:]
     mixb[t, pl.ds(0, TOK)] = mixed[:, :WIDE]
     mixb[t, pl.ds(TOK, 192)] = (dot(mixed[:192], low) + dot(mixed[192:], high)).astype(BF)
     gm.start()
-    gm.near()
-    gm.middle()
-    gm.rest()
+    for _, *way in MIX_ORDER:
+        gm.take(*way)
+    gm.finish()
     for c in loads[:n_out]:
         c.wait()
 
@@ -464,183 +509,176 @@
     nbuf[t] = (res * gain_ref[...]).astype(BF)
     gn.start()
 
+    outgo[...] = dot(pt[...], nbuf[t]).astype(BF)
+
+    def place(p):
+        return pl.ds(pl.multiple_of(p * SLOT, 8), SLOT)
+
+    def both_ways(a, b, op):
+        def step(m, c):
+            op(2 * m - 1, 2 * m, m)
+            op(2 * m, 2 * m - 1, -m)
+            return c
+
+        lax.fori_loop(a, b, step, 0)
+
+    def exchange(src, dst, send, recv):
+        def copy(p, q, k):
+            return pltpu.make_async_remote_copy(
+                src_ref=src.at[place(p)],
+                dst_ref=dst.at[place(q)],
+                send_sem=send.at[p],
+                recv_sem=recv.at[q],
+                device_id={"sp": lax.rem(s + k + NSP, NSP)},
+                device_id_type=MESH,
+            )
+
+        return copy
+
+    go, re = exchange(outgo, arr, go_s, go_r), exchange(back, ret, re_s, re_r)
+    go(31, 31, 16).start()
+
+    def go_start(i, c):
+        m = 16 - i
+        go(2 * m, 2 * m - 1, -m).start()
+        go(2 * m - 1, 2 * m, m).start()
+        return c
+
+    lax.fori_loop(1, 16, go_start, 0)
+    arr[pl.ds(0, SLOT)] = outgo[pl.ds(0, SLOT)]
+
+    def arrived(copy, a, b):
+        def step(p, c):
+            copy(p, p, 1).wait_recv()
+            return c
+
+        lax.fori_loop(a, b, step, 0)
+
+    def spread_sums(buf, send, recv):
+        def step(k, c):
+            pltpu.make_async_remote_copy(
+                src_ref=buf.at[t],
+                dst_ref=buf.at[t],
+                send_sem=send.at[k],
+                recv_sem=recv.at[t],
+                device_id={"tp": lax.rem(t + k, NTP)},
+                device_id_type=MESH,
+            ).start()
+            return c
+
+        lax.fori_loop(1, NTP, step, 0)
+
+    def total_scale(buf, send, recv):
+        def step(k, c):
+            src = lax.rem(t + k, NTP)
+            pltpu.make_async_remote_copy(
+                src_ref=buf.at[t],
+                dst_ref=buf.at[src],
+                send_sem=send.at[k],
+                recv_sem=recv.at[src],
+                device_id={"tp": src},
+                device_id_type=MESH,
+            ).wait_recv()
+            return c
+
+        lax.fori_loop(1, NTP, step, 0)
+        square = buf[0]
+        for j in range(1, NTP):
+            square = square + buf[j]
+        root = lax.rsqrt(square / D + NORM_EPS)
+        return jnp.transpose(jnp.broadcast_to(root, (128, root.shape[1])))
+
     sqb[t] = jnp.sum(jnp.transpose(res * res), axis=0, keepdims=True)
-
-    def sq_start(k, c):
-        pltpu.make_async_remote_copy(
-            src_ref=sqb.at[t],
-            dst_ref=sqb.at[t],
-            send_sem=sq_s.at[k],
-            recv_sem=sq_r.at[t],
-            device_id={"tp": lax.rem(t + k, NTP)},
-            device_id_type=MESH,
-        ).start()
-        return c
-
-    def sq_wait(k, c):
-        src = lax.rem(t + k, NTP)
-        pltpu.make_async_remote_copy(
-            src_ref=sqb.at[t],
-            dst_ref=sqb.at[src],
-            send_sem=sq_s.at[k],
-            recv_sem=sq_r.at[src],
-            device_id={"tp": src},
-            device_id_type=MESH,
-        ).wait_recv()
-        return c
-
-    lax.fori_loop(1, NTP, sq_start, 0)
-    gn.near()
-    lax.fori_loop(1, NTP, sq_wait, 0)
-    square = sqb[0]
-    for j in range(1, NTP):
-        square = square + sqb[j]
-    scale = lax.rsqrt(square / D + NORM_EPS)
-    scale = jnp.transpose(jnp.broadcast_to(scale, (128, TOK)))
-    normed = (resid[...] * scale * gain_ref[...]).astype(BF)
-
-    outgo[...] = dot(pt[...], normed).astype(BF)
-
-    def place(k):
-        return pl.ds(pl.multiple_of(lax.rem(k + 2 * NSP, NSP) * SLOT, 8), SLOT)
-
-    def go_start(k, c):
-        dest = lax.rem(s + k, NSP)
-        pltpu.make_async_remote_copy(
-            src_ref=outgo.at[place(k + 8)],
-            dst_ref=arr.at[place(8 - k)],
-            send_sem=go_s.at[k],
-            recv_sem=go_r.at[lax.rem(NSP - k, NSP)],
-            device_id={"sp": dest},
-            device_id_type=MESH,
-        ).start()
-        return c
-
-    def go_wait(k):
-        pltpu.make_async_remote_copy(
-            src_ref=outgo.at[place(0)],
-            dst_ref=arr.at[place(k + 8)],
-            send_sem=go_s.at[k],
-            recv_sem=go_r.at[k],
-            device_id={"sp": lax.rem(s + k, NSP)},
-            device_id_type=MESH,
-        ).wait_recv()
-
-    def both_ways(a, b, op):
-        def step(k, c):
-            op(k, c)
-            op(NSP - k, c)
-            return c
-
-        lax.fori_loop(a, b, step, 0)
-
-    both_ways(1, 16, go_start)
-    go_start(16, 0)
-    arr[pl.ds(8 * SLOT, SLOT)] = outgo[pl.ds(8 * SLOT, SLOT)]
+    spread_sums(sqb, sq_s, sq_r)
 
     p_i, q_i = iota((PAIR, 2 * SLOT), 0), iota((PAIR, 2 * SLOT), 1)
-    skip = jnp.where(p_i >= 36, SLOT - 36, 0)
-    squeeze = (q_i == p_i + skip).astype(BF)
+    squeeze = (q_i == p_i + jnp.where(p_i >= 36, SLOT - 36, 0)).astype(BF)
     p_i, q_i = iota((2 * SLOT, PAIR), 0), iota((2 * SLOT, PAIR), 1)
-    spread = ((p_i == q_i + jnp.where(q_i >= 36, SLOT - 36, 0))).astype(BF)
+    spread = (p_i == q_i + jnp.where(q_i >= 36, SLOT - 36, 0)).astype(BF)
 
     def pack(c):
-        for k in range(8):
-            rows = arr[pl.ds((c * 8 + k) * 2 * SLOT, 2 * SLOT)]
-            rbuf[t, pl.ds((c * 8 + k) * PAIR, PAIR)] = dot(squeeze, rows).astype(BF)
-
-    def near_wait(k, c):
-        go_wait(k)
-        return c
-
-    gn.middle()
-    gn.rest()
-    for c in loads[n_out:n_shared]:
-        c.wait()
-    lhs = jnp.concatenate([nbuf[j] for j in range(NTP)], axis=1)
-    both = dot(lhs, wsgu[...])
-    hsbuf[t] = (silu(both[:, :128] * scale) * (both[:, 128:] * scale)).astype(BF)
-    gs.start()
-    lax.fori_loop(1, 8, near_wait, 0)
-    lax.fori_loop(24, NSP, near_wait, 0)
-    pack(0)
-    r0.start()
-    gs.near()
-    r0.near()
-    gs.middle()
-    lax.fori_loop(8, 24, near_wait, 0)
-    pack(1)
-    r1.start()
-    r0.middle()
-    gs.rest()
-    r1.near()
-    r0.rest()
-    for c in loads[n_shared:]:
-        c.wait()
+        arrived(go, max(c * 8, 1), c * 8 + 8)
+        for k in range(4):
+            rows = arr[pl.ds((c * 4 + k) * 2 * SLOT, 2 * SLOT)]
+            rbuf[t, pl.ds((c * 4 + k) * PAIR, PAIR)] = dot(squeeze, rows).astype(BF)
+        gr[c].start()
+
+    def squares():
+        mine = rbuf[t].astype(F32) / gain_ref[...]
+        sq2b[t] = jnp.sum(jnp.transpose(mine * mine), axis=0, keepdims=True)
+        spread_sums(sq2b, sq2_s, sq2_r)
+
+    def shared():
+        gn.finish()
+        scale = total_scale(sqb, sq_s, sq_r)
+        for c in loads[n_out:n_shared]:
+            c.wait()
+        lhs = jnp.concatenate([nbuf[j] for j in range(NTP)], axis=1)
+        both = dot(lhs, wsgu[...])
+        hsbuf[t] = (silu(both[:, :128] * scale) * (both[:, 128:] * scale)).astype(BF)
+        gs.start()
+
+    scaled = []
 
     def routed(c):
+        gr[c].finish()
+        if not scaled:
+            sc2[...] = total_scale(sq2b, sq2_s, sq2_r)
+            for w in loads[n_shared:]:
+                w.wait()
+            scaled.append(c)
+
         def step(i, carry):
-            r = pl.ds(pl.multiple_of(c * FAR + i * 192, 8), 192)
+            r = pl.ds(pl.multiple_of(c * CHUNK + i * (CHUNK // 2), 8), CHUNK // 2)
             left = jnp.concatenate([rbuf[j, r] for j in range(NTP)], axis=1)
             both = dot(left, wegu[...])
-            hrbuf[t, r] = (silu(both[:, :128]) * both[:, 128:]).astype(BF)
+            sc = sc2[r]
+            hrbuf[t, r] = (silu(both[:, :128] * sc) * (both[:, 128:] * sc)).astype(BF)
             return carry
 
-        lax.fori_loop(0, FAR // 192, step, 0)
-
-    routed(0)
-    r1.middle()
-    f0.start()
-    r1.rest()
-    routed(1)
-    f1.start()
-    f1.near()
-    f0.near()
-    f1.middle()
-    lhs = jnp.concatenate([hsbuf[j] for j in range(NTP)], axis=1)
-    resid[...] += dot(lhs, wsd[...])
-    f1.rest()
-
-    def re_start(k, c):
-        pltpu.make_async_remote_copy(
-            src_ref=back.at[place(k + 8)],
-            dst_ref=ret.at[place(8 - k)],
-            send_sem=re_s.at[k],
-            recv_sem=re_r.at[lax.rem(NSP - k, NSP)],
-            device_id={"sp": lax.rem(s + k, NSP)},
-            device_id_type=MESH,
-        ).start()
-        return c
-
-    def re_wait(k, c):
-        pltpu.make_async_remote_copy(
-            src_ref=back.at[place(0)],
-            dst_ref=ret.at[place(k + 8)],
-            send_sem=re_s.at[k],
-            recv_sem=re_r.at[k],
-            device_id={"sp": lax.rem(s + k, NSP)},
-            device_id_type=MESH,
-        ).wait_recv()
-        return c
+        lax.fori_loop(0, 2, step, 0)
+        gf[c].start()
+
+    def shared_down():
+        gs.finish()
+        lhs = jnp.concatenate([hsbuf[j] for j in range(NTP)], axis=1)
+        resid[...] += dot(lhs, wsd[...])
 
     def down(c):
-        left = jnp.concatenate([hrbuf[j, pl.ds(c * FAR, FAR)] for j in range(NTP)], axis=1)
+        gf[c].finish()
+        left = jnp.concatenate([hrbuf[j, pl.ds(c * CHUNK, CHUNK)] for j in range(NTP)], axis=1)
         y = dot(left, wed[...]).astype(BF)
-        for k in range(8):
-            back[pl.ds((c * 8 + k) * 2 * SLOT, 2 * SLOT)] = dot(
+        for k in range(4):
+            back[pl.ds((c * 4 + k) * 2 * SLOT, 2 * SLOT)] = dot(
                 spread, y[k * PAIR : (k + 1) * PAIR]
             ).astype(BF)
 
-    down(1)
-    re_start(16, 0)
-    both_ways(9, 16, re_start)
-    re_start(8, 0)
-    f0.middle()
-    f0.rest()
-    down(0)
-    re_start(24, 0)
-    both_ways(1, 8, re_start)
-    ret[pl.ds(8 * SLOT, SLOT)] = back[pl.ds(8 * SLOT, SLOT)]
+    def give(c):
+        if c == 3:
+            re(31, 31, 16).start()
+        else:
+            re(8 * c + 7, 8 * c + 8, 4 * c + 4).start()
+        both_ways(4 * c + 1, 4 * c + 4, lambda p, q, k: re(p, q, k).start())
+        if c:
+            re(8 * c, 8 * c - 1, -4 * c).start()
+
+    for step in ORDER:
+        if not isinstance(step, str):
+            gathers[step[0] + 1].take(*step[1:])
+        elif step == "shared":
+            shared()
+        elif step == "sdown":
+            shared_down()
+        elif step == "sq2":
+            squares()
+        elif step[:4] == "pack":
+            pack(int(step[4]))
+        elif step[:6] == "routed":
+            routed(int(step[6]))
+        else:
+            down(int(step[4]))
+            give(int(step[4]))
+    ret[pl.ds(0, SLOT)] = back[pl.ds(0, SLOT)]
 
     halo_up.wait_send()
     halo_down.wait_send()
@@ -649,26 +687,20 @@
 
     def drain_sp(k, c):
         carry_copy(k).wait_send()
-        for sem in (go_s, re_s):
+        go(k, k, 1).wait_send()
+        re(k, k, 1).wait_send()
+        return c
+
+    def drain_tp(k, c):
+        for buf, send, recv in ((sqb, sq_s, sq_r), (sq2b, sq2_s, sq2_r)):
             pltpu.make_async_remote_copy(
-                src_ref=outgo.at[pl.ds(0, SLOT)],
-                dst_ref=ret.at[pl.ds(0, SLOT)],
-                send_sem=sem.at[k],
-                recv_sem=re_r.at[s],
-                device_id={"sp": lax.rem(s + k, NSP)},
+                src_ref=buf.at[t],
+                dst_ref=buf.at[t],
+                send_sem=send.at[k],
+                recv_sem=recv.at[t],
+                device_id={"tp": lax.rem(t + k, NTP)},
                 device_id_type=MESH,
             ).wait_send()
-        return c
-
-    def drain_tp(k, c):
-        pltpu.make_async_remote_copy(
-            src_ref=sqb.at[t],
-            dst_ref=sqb.at[t],
-            send_sem=sq_s.at[k],
-            recv_sem=sq_r.at[t],
-            device_id={"tp": lax.rem(t + k, NTP)},
-            device_id_type=MESH,
-        ).wait_send()
         return c
 
     weights = rw_ref[...]
@@ -682,10 +714,9 @@
         got = ret[at]
         return w0 * dot(pk0[:, at], got) + w1 * dot(pk1[:, at], got)
 
-    lax.fori_loop(8, 24, re_wait, 0)
+    arrived(re, 16, NSP)
     resid[...] += combine(1)
-    lax.fori_loop(1, 8, re_wait, 0)
-    lax.fori_loop(24, NSP, re_wait, 0)
+    arrived(re, 1, 16)
     out_ref[...] = (resid[...] + combine(0)).astype(BF)
     lax.fori_loop(1, NSP, drain_sp, 0)
 
@@ -715,7 +746,7 @@
     vmem = pl.BlockSpec(memory_space=pltpu.VMEM)
     hbm = pl.BlockSpec(memory_space=pl.ANY)
     dma = pltpu.SemaphoreType.DMA
-    gather_sems = [dma((2, 20)), dma((2, len(RECV)))] * 7
+    gather_sems = [dma((2, 20)), dma((2, len(RECV)))] * 11
     return pl.pallas_call(
         kernel,
         out_shape=jax.ShapeDtypeStruct((TOK, 128), BF),
@@ -739,6 +770,8 @@
             pltpu.VMEM((D, 128), BF),
             pltpu.VMEM((TOK, 128), F32),
             pltpu.VMEM((NTP, 1, TOK), F32),
+            pltpu.VMEM((NTP, 1, DENSE), F32),
+            pltpu.VMEM((DENSE, 128), F32),
             pltpu.VMEM((NTP, TOK, 128), BF),
             pltpu.VMEM((NTP, TOK, 128), BF),
             pltpu.VMEM((NTP, DENSE, 128), BF),
@@ -755,6 +788,8 @@
             dma((2,)),
             dma((NSP,)),
             dma((NSP,)),
+            dma((NTP,)),
+            dma((NTP,)),
             dma((NTP,)),
             dma((NTP,)),
             dma((NSP,)),

time: 157 us -> 148 us (0.943)
  Pallas kernels: 156 us -> 146 us
    pallas_call x1, Pallas kernels: 156 us -> 146 us  [layer(): pl.pallas_call(kernel, out_shape=jax.ShapeDtypeStruct((TOK, 128), BF), in...]
where the time goes in v1:
time: 148 us
  Pallas kernels  146 us (99%)
  local copies, waits for them, and re-layouts  1.54 us (1%)
    pallas_call x1, Pallas kernels, layer(): pl.pallas_call(kernel, out_shape=jax.ShapeDtypeStruct((TOK, 128), BF), in...  146 us

profile of v1, /device:TPU:1, one launch (start us, length us, event | category | flops | bytes accessed | tf_op | source)
XLA Modules:
  0.0 147.5 jit_solution(3226499452247185088)
XLA Ops:
  0.0 146.0 %layer.1 = bf16[384,128]{1,0:T(8,128)(2,1)} custom-call(bf16[192,384]{1,0:T(8,128)(2,1)} %bitcast.18, bf16[192,384]{1,0:T(8,128)(2,1)} %bitcast.19, bf16[4,192]{1,0:T(4,128)(2,1)} %conv_ref.1, bf16[2,128,128]{2,1,0:T(8,128)(2,1)} %bitcast.20, bf16[2,64,64]{2,1,0:T(8,128)(2,1)} %bitcast.22, bf16[2,128,128]{2,1,0:T(8,128)(2,1)} %bitcast.21, ...), custom_call_target="tpu_custom_call" | custom-call | tf_op jit(solution)/shard_map/layer/pallas_call | solution.py:750
  146.0 1.5 %copy.22 = bf16[384,128]{1,0:T(8,128)(2,1)} copy(bf16[384,128]{1,0:T(8,128)(2,1)} %layer.1) | data formatting | bytes 196608

commit v2 on v1

--- a/solution.py
+++ b/solution.py
@@ -59,51 +59,51 @@
     (0, 1, 0, 3, 0), (0, 1, 1, 0, 0), (0, 1, 3, 0, 0), (0, 0, 2, 0, 0), (0, 0, 2, 0, 1),
     (0, 0, 1, 1, 0), (0, 0, 1, 3, 0), (0, 0, 3, 1, 0), (0, 1, 1, 1, 0), (0, 0, 3, 3, 0),
     (0, 1, 1, 3, 0), (0, 1, 2, 0, 0), (0, 1, 2, 0, 1), (0, 1, 3, 1, 0), (0, 1, 3, 3, 0),
-    (0, 0, 2, 1, 0), (0, 0, 2, 3, 0), (0, 1, 2, 1, 0), (0, 1, 2, 3, 0), "pack3", "shared",
-    (5, 0, 0, 1, 0), (5, 0, 0, 3, 0), (5, 0, 1, 0, 0), (5, 0, 3, 0, 0), (5, 1, 0, 1, 0),
-    (5, 1, 0, 3, 0), (5, 1, 1, 0, 0), (5, 1, 3, 0, 0), (1, 0, 0, 1, 0), (1, 0, 0, 3, 0),
-    (1, 0, 1, 0, 0), (1, 0, 3, 0, 0), "pack2", (1, 1, 0, 1, 0), (1, 1, 0, 3, 0), (1, 1, 1, 0, 0),
-    (1, 1, 3, 0, 0), (5, 0, 2, 0, 0), (5, 0, 2, 0, 1), (5, 0, 1, 1, 0), (5, 0, 1, 3, 0), "pack1",
-    (5, 1, 1, 1, 0), (5, 0, 3, 1, 0), (5, 0, 3, 3, 0), (5, 1, 1, 3, 0), (5, 1, 2, 0, 0),
-    (5, 1, 2, 0, 1), (5, 1, 3, 1, 0), (5, 1, 3, 3, 0), "pack0", (1, 0, 2, 0, 0), (1, 0, 2, 0, 1),
-    "sq2", (1, 0, 1, 1, 0), (1, 0, 1, 3, 0), (4, 0, 1, 0, 0), (4, 0, 3, 0, 0), (4, 1, 0, 1, 0),
-    (4, 1, 0, 3, 0), (1, 0, 3, 1, 0), (1, 0, 3, 3, 0), (4, 0, 0, 1, 0), (4, 0, 0, 3, 0),
-    (1, 1, 1, 1, 0), (1, 1, 1, 3, 0), (4, 1, 1, 0, 0), (4, 1, 3, 0, 0), (1, 1, 2, 0, 0),
-    (1, 1, 2, 0, 1), (1, 1, 3, 1, 0), (1, 1, 3, 3, 0), (5, 0, 2, 1, 0), (5, 0, 2, 3, 0),
-    (3, 0, 1, 0, 0), (3, 0, 3, 0, 0), (3, 1, 0, 1, 0), (3, 0, 0, 1, 0), (3, 0, 0, 3, 0),
-    (3, 1, 0, 3, 0), (3, 1, 1, 0, 0), (3, 1, 3, 0, 0), (5, 1, 2, 1, 0), (5, 1, 2, 3, 0),
-    (2, 0, 0, 1, 0), (2, 0, 0, 3, 0), (2, 0, 1, 0, 0), (2, 0, 3, 0, 0), (2, 1, 1, 0, 0),
-    (2, 1, 3, 0, 0), (2, 1, 0, 1, 0), (2, 1, 0, 3, 0), (4, 0, 2, 0, 0), (4, 0, 2, 0, 1),
-    (1, 0, 2, 1, 0), (1, 0, 2, 3, 0), (4, 0, 1, 1, 0), (4, 0, 1, 3, 0), (4, 1, 1, 1, 0),
-    (4, 1, 1, 3, 0), (4, 0, 3, 1, 0), (4, 0, 3, 3, 0), (4, 1, 3, 1, 0), (4, 1, 3, 3, 0),
-    (1, 1, 2, 1, 0), (1, 1, 2, 3, 0), (4, 1, 2, 0, 0), (4, 1, 2, 0, 1), (3, 0, 2, 0, 0),
-    (3, 0, 2, 0, 1), (3, 0, 1, 1, 0), (3, 0, 1, 3, 0), (3, 1, 1, 1, 0), (3, 0, 3, 1, 0),
-    (3, 0, 3, 3, 0), (3, 1, 1, 3, 0), (3, 1, 3, 1, 0), (3, 1, 2, 0, 0), (3, 1, 2, 0, 1),
+    (0, 0, 2, 1, 0), (0, 0, 2, 3, 0), (0, 1, 2, 1, 0), (0, 1, 2, 3, 0), "shared", "pack3",
+    (1, 0, 0, 1, 0), (1, 0, 0, 3, 0), (1, 0, 1, 0, 0), (1, 0, 3, 0, 0), (1, 1, 0, 1, 0),
+    (1, 1, 0, 3, 0), (1, 1, 1, 0, 0), (1, 1, 3, 0, 0), "pack2", (5, 0, 0, 1, 0), (5, 0, 0, 3, 0),
+    (5, 0, 1, 0, 0), (5, 0, 3, 0, 0), (5, 1, 0, 1, 0), (5, 1, 0, 3, 0), (5, 1, 1, 0, 0),
+    (5, 1, 3, 0, 0), (1, 0, 2, 0, 0), (1, 0, 2, 0, 1), (1, 0, 1, 1, 0), (1, 0, 1, 3, 0),
+    (1, 0, 3, 1, 0), (1, 1, 1, 1, 0), (1, 0, 3, 3, 0), (1, 1, 1, 3, 0), (1, 1, 2, 0, 0),
+    (1, 1, 2, 0, 1), (1, 1, 3, 1, 0), (1, 1, 3, 3, 0), (4, 0, 0, 1, 0), (4, 0, 0, 3, 0),
+    (4, 0, 1, 0, 0), (4, 0, 3, 0, 0), (4, 1, 1, 0, 0), (4, 1, 3, 0, 0), (4, 1, 0, 1, 0),
+    (4, 1, 0, 3, 0), (5, 0, 2, 0, 0), (5, 0, 2, 0, 1), (5, 0, 1, 1, 0), (5, 0, 1, 3, 0),
+    (5, 0, 3, 1, 0), (5, 0, 3, 3, 0), (5, 1, 1, 1, 0), (5, 1, 1, 3, 0), "pack1", (5, 1, 2, 0, 0),
+    (5, 1, 2, 0, 1), (5, 1, 3, 1, 0), (5, 1, 3, 3, 0), (1, 0, 2, 1, 0), (1, 0, 2, 3, 0),
+    (1, 1, 2, 1, 0), (1, 1, 2, 3, 0), (4, 0, 2, 0, 0), (4, 0, 2, 0, 1), (4, 0, 1, 1, 0),
+    (4, 0, 1, 3, 0), (4, 1, 1, 1, 0), (4, 1, 1, 3, 0), (4, 0, 3, 1, 0), (4, 0, 3, 3, 0),
+    (4, 1, 2, 0, 0), (4, 1, 2, 0, 1), (4, 1, 3, 1, 0), (4, 1, 3, 3, 0), "pack0", "sq2",
+    (5, 0, 2, 1, 0), (5, 0, 2, 3, 0), (3, 0, 1, 0, 0), (3, 0, 3, 0, 0), (3, 0, 0, 1, 0),
+    (3, 0, 0, 3, 0), (3, 1, 0, 1, 0), (3, 1, 0, 3, 0), (3, 1, 1, 0, 0), (3, 1, 3, 0, 0),
+    (5, 1, 2, 1, 0), (5, 1, 2, 3, 0), "sdown", (4, 0, 2, 1, 0), (4, 0, 2, 3, 0), (4, 1, 2, 1, 0),
+    (4, 1, 2, 3, 0), (2, 0, 0, 1, 0), (2, 0, 0, 3, 0), (2, 0, 1, 0, 0), (2, 0, 3, 0, 0),
+    (2, 1, 1, 0, 0), (2, 1, 3, 0, 0), (2, 1, 0, 1, 0), (2, 1, 0, 3, 0), (3, 0, 2, 0, 0),
+    (3, 0, 2, 0, 1), (3, 0, 1, 1, 0), (3, 0, 1, 3, 0), (3, 0, 3, 1, 0), (3, 0, 3, 3, 0),
+    (3, 1, 1, 1, 0), (3, 1, 1, 3, 0), (3, 1, 2, 0, 0), (3, 1, 2, 0, 1), (3, 1, 3, 1, 0),
     (3, 1, 3, 3, 0), "routed3", (2, 0, 2, 0, 0), (2, 0, 2, 0, 1), (2, 0, 1, 1, 0), (2, 0, 1, 3, 0),
-    (2, 1, 1, 1, 0), (2, 1, 1, 3, 0), (2, 0, 3, 1, 0), (2, 0, 3, 3, 0), (2, 1, 3, 1, 0),
-    (2, 1, 2, 0, 0), (2, 1, 2, 0, 1), (2, 1, 3, 3, 0), (4, 0, 2, 1, 0), (4, 0, 2, 3, 0), "sdown",
-    (4, 1, 2, 1, 0), (4, 1, 2, 3, 0), (3, 0, 2, 1, 0), (3, 0, 2, 3, 0), (3, 1, 2, 3, 0),
-    (3, 1, 2, 1, 0), (9, 0, 0, 1, 0), (9, 0, 0, 3, 0), (9, 0, 1, 0, 0), (9, 0, 3, 0, 0),
-    (9, 1, 1, 0, 0), (9, 1, 3, 0, 0), (9, 1, 0, 1, 0), (9, 1, 0, 3, 0), (2, 0, 2, 1, 0),
-    (2, 0, 2, 3, 0), (2, 1, 2, 3, 0), (2, 1, 2, 1, 0), "routed2", (9, 0, 2, 0, 0), (9, 0, 2, 0, 1),
-    "routed1", (9, 0, 1, 1, 0), (9, 0, 1, 3, 0), (9, 1, 1, 1, 0), (9, 1, 1, 3, 0), (9, 0, 3, 1, 0),
-    (9, 0, 3, 3, 0), (9, 1, 3, 1, 0), (9, 1, 2, 0, 0), (9, 1, 2, 0, 1), (9, 1, 3, 3, 0), "routed0",
-    (8, 0, 0, 1, 0), (8, 0, 0, 3, 0), (8, 0, 1, 0, 0), (8, 0, 3, 0, 0), (8, 1, 0, 1, 0),
-    (8, 1, 0, 3, 0), (8, 1, 1, 0, 0), (8, 1, 3, 0, 0), (7, 0, 1, 0, 0), (7, 0, 3, 0, 0),
-    (9, 0, 2, 1, 0), (9, 0, 2, 3, 0), (7, 0, 0, 1, 0), (7, 0, 0, 3, 0), (7, 1, 0, 1, 0),
-    (7, 1, 0, 3, 0), (7, 1, 1, 0, 0), (7, 1, 3, 0, 0), (9, 1, 2, 3, 0), (9, 1, 2, 1, 0),
-    (6, 0, 0, 1, 0), (6, 0, 0, 3, 0), (6, 0, 1, 0, 0), (6, 0, 3, 0, 0), (6, 1, 0, 1, 0),
-    (6, 1, 0, 3, 0), (6, 1, 1, 0, 0), (6, 1, 3, 0, 0), (8, 0, 2, 0, 0), (8, 0, 2, 0, 1),
-    (8, 0, 1, 1, 0), (8, 0, 1, 3, 0), (8, 1, 1, 1, 0), (8, 1, 1, 3, 0), (8, 0, 3, 1, 0),
-    (8, 0, 3, 3, 0), (8, 1, 2, 0, 0), (8, 1, 2, 0, 1), (8, 1, 3, 1, 0), (8, 1, 3, 3, 0),
-    (7, 0, 2, 0, 0), (7, 0, 2, 0, 1), (7, 0, 1, 1, 0), (7, 0, 1, 3, 0), (7, 0, 3, 1, 0),
-    (7, 0, 3, 3, 0), (7, 1, 1, 1, 0), (7, 1, 1, 3, 0), (7, 1, 3, 1, 0), (7, 1, 3, 3, 0),
-    (7, 1, 2, 0, 0), (7, 1, 2, 0, 1), "down3", (6, 0, 2, 0, 0), (6, 0, 2, 0, 1), (6, 0, 1, 1, 0),
-    (6, 0, 1, 3, 0), (6, 1, 1, 1, 0), (6, 1, 1, 3, 0), (6, 0, 3, 1, 0), (6, 0, 3, 3, 0),
-    (6, 1, 2, 0, 0), (6, 1, 2, 0, 1), (6, 1, 3, 1, 0), (6, 1, 3, 3, 0), (8, 0, 2, 1, 0),
-    (8, 0, 2, 3, 0), (8, 1, 2, 1, 0), (8, 1, 2, 3, 0), (7, 0, 2, 1, 0), (7, 0, 2, 3, 0),
-    (7, 1, 2, 1, 0), (7, 1, 2, 3, 0), (6, 0, 2, 1, 0), (6, 0, 2, 3, 0), (6, 1, 2, 1, 0),
-    (6, 1, 2, 3, 0), "down2", "down1", "down0",
+    "routed2", (2, 1, 1, 1, 0), (2, 1, 1, 3, 0), (2, 0, 3, 1, 0), (2, 0, 3, 3, 0), (2, 1, 2, 0, 0),
+    (2, 1, 2, 0, 1), (2, 1, 3, 1, 0), (2, 1, 3, 3, 0), (3, 0, 2, 1, 0), (3, 0, 2, 3, 0),
+    (3, 1, 2, 1, 0), (3, 1, 2, 3, 0), (9, 0, 0, 1, 0), (9, 0, 0, 3, 0), (9, 0, 1, 0, 0),
+    (9, 0, 3, 0, 0), (9, 1, 1, 0, 0), (9, 1, 3, 0, 0), (9, 1, 0, 1, 0), (9, 1, 0, 3, 0),
+    (2, 0, 2, 1, 0), (2, 0, 2, 3, 0), (8, 0, 1, 0, 0), (8, 0, 3, 0, 0), (8, 0, 0, 1, 0),
+    (8, 0, 0, 3, 0), (8, 1, 0, 1, 0), (8, 1, 0, 3, 0), (8, 1, 1, 0, 0), (8, 1, 3, 0, 0),
+    (2, 1, 2, 1, 0), (2, 1, 2, 3, 0), "routed1", (9, 0, 2, 0, 0), (9, 0, 2, 0, 1), (9, 0, 1, 1, 0),
+    (9, 0, 1, 3, 0), (9, 1, 1, 1, 0), (9, 1, 1, 3, 0), (9, 0, 3, 1, 0), (9, 0, 3, 3, 0),
+    (9, 1, 2, 0, 0), (9, 1, 2, 0, 1), (9, 1, 3, 1, 0), (9, 1, 3, 3, 0), (8, 0, 2, 0, 0),
+    (8, 0, 2, 0, 1), (8, 0, 1, 1, 0), (8, 0, 1, 3, 0), (8, 0, 3, 1, 0), (8, 0, 3, 3, 0),
+    (8, 1, 1, 1, 0), (8, 1, 1, 3, 0), (8, 1, 2, 0, 0), (8, 1, 2, 0, 1), (8, 1, 3, 1, 0),
+    (8, 1, 3, 3, 0), "routed0", (7, 0, 0, 1, 0), (7, 0, 0, 3, 0), (7, 0, 1, 0, 0), (7, 0, 3, 0, 0),
+    (7, 1, 1, 0, 0), (7, 1, 3, 0, 0), (7, 1, 0, 1, 0), (7, 1, 0, 3, 0), (9, 0, 2, 1, 0),
+    (9, 0, 2, 3, 0), (9, 1, 2, 1, 0), (9, 1, 2, 3, 0), (8, 0, 2, 1, 0), (8, 0, 2, 3, 0),
+    (8, 1, 2, 1, 0), (8, 1, 2, 3, 0), (6, 0, 0, 1, 0), (6, 0, 0, 3, 0), (6, 0, 1, 0, 0),
+    (6, 0, 3, 0, 0), (6, 1, 1, 0, 0), (6, 1, 3, 0, 0), (6, 1, 0, 1, 0), (6, 1, 0, 3, 0),
+    (7, 0, 2, 0, 0), (7, 0, 2, 0, 1), (7, 0, 1, 1, 0), (7, 0, 1, 3, 0), (7, 1, 1, 1, 0),
+    (7, 1, 1, 3, 0), (7, 0, 3, 1, 0), (7, 0, 3, 3, 0), (7, 1, 2, 0, 0), (7, 1, 2, 0, 1),
+    (7, 1, 3, 1, 0), (7, 1, 3, 3, 0), "down3", (6, 0, 2, 0, 0), (6, 0, 2, 0, 1), "down2",
+    (6, 0, 1, 1, 0), (6, 0, 1, 3, 0), (6, 1, 1, 1, 0), (6, 1, 1, 3, 0), (6, 0, 3, 1, 0),
+    (6, 0, 3, 3, 0), (6, 1, 2, 0, 0), (6, 1, 2, 0, 1), (6, 1, 3, 1, 0), (6, 1, 3, 3, 0),
+    (7, 0, 2, 1, 0), (7, 0, 2, 3, 0), (7, 1, 2, 1, 0), (7, 1, 2, 3, 0), (6, 0, 2, 1, 0),
+    (6, 0, 2, 3, 0), (6, 1, 2, 1, 0), (6, 1, 2, 3, 0), "down1", "down0",
 )
 
 
@@ -336,21 +336,11 @@
         low = (left - mid.astype(F32)).astype(BF)
         av[d] = (dot(order, high, 1, 1) + dot(order, mid, 1, 1)) + dot(order, low, 1, 1)
 
-    halo_up.wait_recv()
-    halo_down.wait_recv()
-    sub = iota((8, CH), 0)
-    first, last = s == 0, s == NSP - 1
-    for k in range(2):
-        edge = jnp.where(first, 0.0, hl[pl.ds(k * 8 + 7, 1)])
-        rolled = pltpu.roll(rp[pl.ds(16 + (46 + k) * 8, 8)], 1, 0)
-        rp[pl.ds(k * 8, 8)] = jnp.where(sub == 0, edge, rolled)
-    edge = jnp.where(last, 0.0, hr[pl.ds(0, 1)])
-    rolled = pltpu.roll(rp[pl.ds(16, 8)], 7, 0)
-    rp[pl.ds(16 + TOK, 8)] = jnp.where(sub == 7, edge, rolled)
     taps = conv_ref[...].astype(F32)
 
     block = 64
-    for i in range(TOK // block):
+
+    def gates(i):
         r0 = i * block
         conv = rp[pl.ds(r0, block)] * taps[0:1]
         for j in range(1, 4):
@@ -369,6 +359,22 @@
             drive = jnp.sqrt(neg_expm1(2.0 * log_decay)) * admit * conv_f
             av[d, pl.ds(r0, block)] = jnp.exp(log_decay)
             bv[d, pl.ds(r0, block)] = drive
+
+    for i in range(1, 5):
+        gates(i)
+    halo_up.wait_recv()
+    halo_down.wait_recv()
+    sub = iota((8, CH), 0)
+    first, last = s == 0, s == NSP - 1
+    for k in range(2):
+        edge = jnp.where(first, 0.0, hl[pl.ds(k * 8 + 7, 1)])
+        rolled = pltpu.roll(rp[pl.ds(16 + (46 + k) * 8, 8)], 1, 0)
+        rp[pl.ds(k * 8, 8)] = jnp.where(sub == 0, edge, rolled)
+    edge = jnp.where(last, 0.0, hr[pl.ds(0, 1)])
+    rolled = pltpu.roll(rp[pl.ds(16, 8)], 7, 0)
+    rp[pl.ds(16 + TOK, 8)] = jnp.where(sub == 7, edge, rolled)
+    gates(0)
+    gates(5)
 
     def scan(i, carry):
         c0, s0, c1, s1 = carry
@@ -604,7 +610,7 @@
         gr[c].start()
 
     def squares():
-        mine = rbuf[t].astype(F32) / gain_ref[...]
+        mine = rbuf[t].astype(F32) * (1.0 / gain_ref[...])
         sq2b[t] = jnp.sum(jnp.transpose(mine * mine), axis=0, keepdims=True)
         spread_sums(sq2b, sq2_s, sq2_r)
 

time: 148 us -> 146 us (0.986)
  Pallas kernels: 146 us -> 144 us
    pallas_call x1, Pallas kernels: 146 us -> 144 us  [layer(): pl.pallas_call(kernel, out_shape=jax.ShapeDtypeStruct((TOK, 128), BF), in...]
where the time goes in v2:
time: 146 us; the launch traced here: 145 us
  Pallas kernels  144 us (99%)
  local copies, waits for them, and re-layouts  1.54 us (1%)
    pallas_call x1, Pallas kernels, layer(): pl.pallas_call(kernel, out_shape=jax.ShapeDtypeStruct((TOK, 128), BF), in...  144 us

profile of v2, /device:TPU:1, one launch (start us, length us, event | category | flops | bytes accessed | tf_op | source)
XLA Modules:
  0.0 145.4 jit_solution(15403053660697041538)
XLA Ops:
  0.0 143.8 %layer.1 = bf16[384,128]{1,0:T(8,128)(2,1)} custom-call(bf16[192,384]{1,0:T(8,128)(2,1)} %bitcast.18, bf16[192,384]{1,0:T(8,128)(2,1)} %bitcast.19, bf16[4,192]{1,0:T(4,128)(2,1)} %conv_ref.1, bf16[2,128,128]{2,1,0:T(8,128)(2,1)} %bitcast.20, bf16[2,64,64]{2,1,0:T(8,128)(2,1)} %bitcast.22, bf16[2,128,128]{2,1,0:T(8,128)(2,1)} %bitcast.21, ...), custom_call_target="tpu_custom_call" | custom-call | tf_op jit(solution)/shard_map/layer/pallas_call | solution.py:756
  143.8 1.5 %copy.22 = bf16[384,128]{1,0:T(8,128)(2,1)} copy(bf16[384,128]{1,0:T(8,128)(2,1)} %layer.1) | data formatting | bytes 196608
